TPU v7x, 32 devices: a whole 2x2x4 slice. The times are simulated.
32 devices in a mesh: grp: 2 (over x), ep: 16 (over z, y, core).
Axes of the slice: x: 2, y: 2, z: 4, core: 2. Of those that a mesh axis runs over, the one named last changes fastest.
Arguments:
- tokens: bfloat16 [2048, 2048], P(('grp', 'ep')), parts along dimension 0, may hold values from -6 to 6
- lengths: int32 [256], P(('grp', 'ep')), parts along dimension 0, may hold values from 1 to 8, 384 in all
- experts: int32 [2048, 2], P(('grp', 'ep')), parts along dimension 0, may hold values from 0 to 3, all different within a row; in each aligned block of 64 rows (0 to 63, 64 to 127, ...) at most 64 rows name the same one
- route_weights: float32 [2048, 2], P(('grp', 'ep')), parts along dimension 0, may hold values from 0.2 to 1
- gate_proj: bfloat16 [16, 2048, 1792], P('ep'), may hold values from -0.125 to 0.125
- up_proj: bfloat16 [16, 2048, 1792], P('ep'), may hold values from -0.125 to 0.125
- down_proj: bfloat16 [16, 1792, 2048], P('ep'), may hold values from -0.0625 to 0.0625
- norm_gain: float32 [2048], replicated, may hold values from 0.1 to 1.9
- norm_bias: float32 [2048], replicated, may hold values from -3 to 3
Outputs:
- mixed: bfloat16 [2048, 2048], P(('grp', 'ep')), parts along dimension 0
There are 2 independent parts, one for each index of `grp`. A program takes and returns all parts, laid end to end along the dimension named above; an argument that names none is the same for every part. Nothing has to cross between parts.
Inputs may be any that keep to these rules, and one draw needn't show every extreme that they name: Each row names 2 different experts; in the rows of one device (aligned blocks of 64 rows) no expert is named by more than 64 rows. Within each copy of the problem the 128 lengths sum to 384; the whole array, over all copies, sums to that times the number of copies.
All inputs are finite; a program needn't handle non-finite values. No bound on the sum of `lengths` on one device may be relied on, other than what follows from the above.
Results may differ from a plain program's by a relative error of at most 0.0021.
Values may be sent and summed in bfloat16 or wider, within the bound.
A program may use at most 128 MiB of HBM per device.

v0:
```python
import jax
import jax.numpy as jnp
from jax import lax
from jax.sharding import PartitionSpec as P

SPLIT = 4
TOP = 2
SPAN = 8


RESIDUAL_SCALE = 8.0**0.25
NORM_EPS = 1e-05


def layer_norm(values, norm_gain, norm_bias):
    center = values - jnp.mean(values, -1, keepdims=True)
    variance = jnp.mean(center * center, -1, keepdims=True)
    return center * lax.rsqrt(variance + NORM_EPS) * norm_gain + norm_bias


def expert_rows(picked, gate_proj, up_proj, down_proj):
    pre_gate = jnp.dot(picked, gate_proj[0], preferred_element_type=jnp.float32)
    pre_up = jnp.dot(picked, up_proj[0], preferred_element_type=jnp.float32)
    hidden = (jax.nn.silu(pre_gate) * pre_up).astype(jnp.bfloat16)
    return jnp.dot(hidden, down_proj[0], preferred_element_type=jnp.float32)


def local(
    tokens, lengths, experts, route_weights, gate_proj, up_proj, down_proj, norm_gain, norm_bias
):
    slot_count, width = tokens.shape
    axis_count = lax.axis_size("ep")
    capacity = 2 * slot_count * TOP * SPLIT // axis_count
    position = jnp.arange(slot_count, dtype=jnp.int32)
    alive_mask = position % SPAN < jnp.repeat(lengths, SPAN, total_repeat_length=slot_count)
    inputs = tokens.astype(jnp.float32)
    gathered = lax.all_gather(tokens, "ep", axis=0, tiled=True)
    all_experts, all_lengths = (
        lax.all_gather(experts, "ep", axis=0, tiled=True),
        lax.all_gather(lengths, "ep", axis=0, tiled=True),
    )
    all_weights = lax.all_gather(route_weights, "ep", axis=0, tiled=True)
    total_slots = gathered.shape[0]
    all_position = jnp.arange(total_slots, dtype=jnp.int32)
    all_alive = all_position % SPAN < jnp.repeat(all_lengths, SPAN, total_repeat_length=total_slots)
    own_expert = lax.axis_index("ep") // SPLIT
    hits = (all_experts == own_expert) & all_alive[:, None]
    chosen = hits.reshape(total_slots * TOP).astype(jnp.int32)
    order_rank = jnp.cumsum(chosen) - 1
    row_count = axis_count * capacity
    rows_index = jnp.arange(row_count, dtype=jnp.int32)
    picker = (order_rank[None, :] == rows_index[:, None]) & (chosen[None, :] == 1)
    flat_slot = jnp.repeat(all_position, TOP, total_repeat_length=total_slots * TOP)
    row_source = jnp.sum(jnp.where(picker, flat_slot[None, :], 0), axis=1)
    picked = jnp.take(gathered, row_source, axis=0)
    results = expert_rows(picked, gate_proj, up_proj, down_proj)
    rank_pairs = order_rank.reshape(total_slots, TOP)
    slot_row = jnp.sum(jnp.where(hits, rank_pairs, 0), axis=1)
    slot_weight = jnp.sum(jnp.where(hits, all_weights, 0.0), axis=1)
    spread_back = jnp.take(results, slot_row, axis=0) * slot_weight[:, None]
    branch = lax.psum_scatter(spread_back, "ep", scatter_dimension=0, tiled=True)
    normed = layer_norm(RESIDUAL_SCALE * inputs + branch, norm_gain, norm_bias)
    return jnp.where(alive_mask[:, None], normed, 0.0).astype(jnp.bfloat16)


def solution(mesh):
    in_specs = (
        P(("grp", "ep"), None),
        P(("grp", "ep")),
        P(("grp", "ep"), None),
        P(("grp", "ep"), None),
        P("ep", None, None),
        P("ep", None, None),
        P("ep", None, None),
        P(),
        P(),
    )
    out_specs = P(("grp", "ep"), None)
    return jax.shard_map(local, mesh=mesh, in_specs=in_specs, out_specs=out_specs, check_vma=False)
```

profile of v0, /device:TPU:0, one launch (start us, length us, event | category | flops | bytes accessed | tf_op | source)
XLA Modules:
  0.0 260.8 jit_solution(14044084314716863981)
XLA Ops:
  6.5 0.0 all-gather.4.cloned.1.call-start
  6.5 0.7 all-gather.4.cloned.1.call-update
  7.3 0.0 reduce-scatter.2.cloned.1.call-start
  7.3 23.6 %all-gather = s32[16,64,2]{1,2,0:T(2,128)S(1)} all-gather(s32[1,64,2]{1,2,0:T(2,128)} %bitcast.52), channel_id=1, replica_groups=mesh['grp'=2,'ep'=16] {'ep'}, dimensions={0}, use_global_device_ids=true | all-gather | bytes 8704 | tf_op jit(solution)/shard_map/all_gather | solution.py:39
  30.9 0.1 reshape.405
  31.0 1.2 dynamic-slice.18
  32.9 0.9 dynamic-update-slice.8
  33.8 7.1 %all-reduce = s32[128]{0:T(128)S(1)} all-reduce(s32[128]{0:T(128)S(1)} %dynamic-update-slice.8), channel_id=1, replica_groups=mesh['grp'=2,'ep'=16] {'ep'}, use_global_device_ids=true, to_apply=%add | all-reduce | flops 128 | bytes 1024
  40.9 0.8 add_add_fusion.1
  41.7 6.6 %gather_fusion = s32[1024]{0:T(1024)S(1)} fusion(s32[128]{0:T(128)S(1)} %all-reduce, s32[1024]{0:T(1024)S(1)} %broadcast_clamp_fusion.2), kind=kCustom, calls=%fused_computation | custom fusion | bytes 12288 | tf_op jit(solution)/shard_map/jit(_take)/gather | solution.py:45
  48.3 0.8 fusion.12
  49.0 0.2 copy.26
  49.3 0.3 reshape.357
  49.5 0.3 reduce-window.23
  49.8 0.1 slice.72
  49.9 0.5 reshape.354
  50.4 23.2 %all-gather.1 = f32[16,64,2]{1,2,0:T(2,128)S(1)} all-gather(f32[1,64,2]{1,2,0:T(2,128)} %bitcast.53), channel_id=1, replica_groups=mesh['grp'=2,'ep'=16] {'ep'}, dimensions={0}, use_global_device_ids=true | all-gather | bytes 8704 | tf_op jit(solution)/shard_map/all_gather | solution.py:42
  73.6 0.1 reshape.403
  73.7 0.3 copy.28
  73.9 0.4 eq.44
  74.3 0.1 slice_reduce_fusion
  74.4 0.1 broadcast.380
  74.5 0.1 reshape.356
  74.6 0.2 copy.27
  74.9 0.1 add_bitcast_fusion
  74.9 2.5 select_reduce_fusion
  77.5 0.0 all-gather.4.cloned.1.call-done
  77.5 11.7 %gather_fusion.1 = bf16[1024,2048]{1,0:T(8,128)(2,1)} fusion(bf16[1024,2048]{1,0:T(8,128)(2,1)} %all-gather.4.cloned.1.call-done, s32[1024]{0:T(1024)S(1)} %broadcast_clamp_fusion.1), kind=kCustom, calls=%fused_computation.1 | custom fusion | bytes 8392704 | tf_op jit(solution)/shard_map/jit(_take)/gather | solution.py:55
  89.3 13.9 %fusion.5 = f32[1024,1792]{1,0:T(8,128)} fusion(bf16[1,2048,1792]{2,1,0:T(8,128)(2,1)} %param.19, bf16[1024,2048]{1,0:T(8,128)(2,1)} %gather_fusion.1, pred[1024]{0:T(1024)(128)(4,1)S(1)} %compare_and_fusion), kind=kOutput, calls=%fused_computation.11 | convolution fusion | flops 7518289920 | bytes 18875392 | tf_op jit(solution)/shard_map/dot_general | solution.py:22
  103.1 26.9 %fusion.1 = f32[1024,2048]{1,0:T(8,128)} fusion(bf16[1,1792,2048]{2,1,0:T(8,128)(2,1)} %param.21, f32[1024,1792]{1,0:T(8,128)} %fusion.5, bf16[1,2048,1792]{2,1,0:T(8,128)(2,1)} %param.20, bf16[1024,2048]{1,0:T(8,128)(2,1)} %gather_fusion.1, pred[1024]{0:T(1024)(128)(4,1)S(1)} %compare_and_fusion), kind=kOutput, calls=%fused_computation.7 | convolution fusion | flops 15045492736 | bytes 34604032 | tf_op jit(solution)/shard_map/dot_general | solution.py:25
  130.1 12.5 %gather_fusion.2 = f32[1024,2048]{1,0:T(8,128)} fusion(f32[1024,2048]{1,0:T(8,128)} %fusion.1, s32[1024]{0:T(1024)S(1)} %broadcast_clamp_fusion), kind=kCustom, calls=%fused_computation.2 | custom fusion | bytes 16781312 | tf_op jit(solution)/shard_map/jit(_take)/gather | solution.py:60
  142.5 6.0 %select_multiply_fusion = f32[1024,2048]{1,0:T(8,128)} fusion(f32[1024,2048]{1,0:T(8,128)} %gather_fusion.2, f32[1024]{0:T(1024)S(1)} %select_reduce_fusion.1, pred[1024]{0:T(1024)(128)(4,1)S(1)} %compare_and_fusion.1), kind=kLoop, calls=%fused_computation.3 | loop fusion | flops 4194304 | bytes 16782336 | tf_op jit(solution)/shard_map/mul | solution.py:60
  148.5 0.0 copy-start.7
  148.5 0.0 copy-start.8
  148.5 0.0 copy-start.9
  148.5 0.0 copy-start.10
  148.6 0.0 copy-start
  148.6 0.0 copy-start.2
  148.6 0.0 copy-start.3
  148.6 0.0 reduce-scatter.2.cloned.1.call-update
  148.6 0.5 copy-done.1
  149.1 0.7 fusion.22
  149.8 0.0 copy-done.4
  149.9 5.1 %fusion.16 = pred[64]{0:T(512)(128)(4,1)S(1)} fusion(pred[64]{0:T(512)(128)(4,1)S(1)} %copy-done.10, pred[64]{0:T(512)(128)(4,1)S(1)} %copy-done.9, pred[64]{0:T(512)(128)(4,1)S(1)} %copy-done.8, pred[64]{0:T(512)(128)(4,1)S(1)} %copy-done.7, pred[64]{0:T(512)(128)(4,1)S(1)} %copy-done.6, pred[64]{0:T(512)(128)(4,1)S(1)} %copy-done.5, ...), kind=kLoop, calls=%fused_computation.46 | loop fusion | flops 896 | bytes 544 | tf_op jit(solution)/shard_map/lt | solution.py:35
  154.9 94.5 %reduce-scatter.2.cloned.1.call-done = f32[64,2048]{1,0:T(8,128)} async-done(((f32[1024,2048]{1,0:T(8,128)}), f32[64,2048]{1,0:T(8,128)}) %reduce-scatter.2.cloned.1.call-update) | async-done | bytes 524304 | tf_op jit(solution)/shard_map/reduce_scatter | solution.py:61
  249.5 1.2 fusion.11
  250.7 1.3 multiply_reduce_fusion
  252.0 1.9 select_convert_fusion
  (31 shorter events, 0.2 us)
Async XLA Ops:
  6.5 71.0 %all-gather.4.cloned.1.call-start = ((), (), s32[]{:S(2)}) async-start(), calls=%async_computation.1 | async-start | bytes 4456448 | tf_op jit(solution)/shard_map/all_gather | solution.py:37
  7.3 242.2 %reduce-scatter.2.cloned.1.call-start = ((), (), s32[]{:S(2)}) async-start(), calls=%async_computation.2 | async-start | bytes 8912896 | tf_op jit(solution)/shard_map/reduce_scatter | solution.py:61
  148.5 0.7 copy-start.1
  148.5 1.3 copy-start.4
  148.5 1.3 copy-start.5
  148.5 1.3 copy-start.6
  148.5 1.3 copy-start.7
  148.5 1.3 copy-start.8
  148.5 1.3 copy-start.9
  148.5 1.3 copy-start.10
  148.6 100.9 %copy-start = (bf16[64,2048]{1,0:T(8,128)(2,1)S(1)}, bf16[64,2048]{1,0:T(8,128)(2,1)}, u32[]{:S(2)}) copy-start(bf16[64,2048]{1,0:T(8,128)(2,1)} %param.15) | copy-start | bytes 786436
  148.6 103.4 %copy-start.2 = (f32[2048]{0:T(1024)S(1)}, f32[2048]{0:T(1024)}, u32[]{:S(2)}) copy-start(f32[2048]{0:T(1024)} %param.23) | copy-start | bytes 24580
  148.6 103.4 %copy-start.3 = (f32[2048]{0:T(1024)S(1)}, f32[2048]{0:T(1024)}, u32[]{:S(2)}) copy-start(f32[2048]{0:T(1024)} %param.22) | copy-start | bytes 24580
Sparse Core Ops, SparseCore 0:
  9.5 53.3 all-gather.3
  148.7 100.6 reduce-scatter.1
where the time goes:
time: 261 us
  waiting for transfers between devices  95.3 us (37%)
  blocking collectives  53.9 us (21%)
  matrix products  40.8 us (16%)
  local copies, waits for them, and re-layouts  36.4 us (14%)
  other arithmetic  20 us (8%)
  between operations  14.3 us (5%)
    reduce_scatter x1, waiting for transfers between devices, local(): lax.psum_scatter(spread_back, 'ep', scatter_dimension=0, tiled=True)  94.5 us
    dot_general x1, matrix products, expert_rows(): return jnp.dot(hidden, down_proj[0], preferred_element_type=jnp.float32)  26.9 us
    all_gather x1, blocking collectives, local(): lax.all_gather(experts, 'ep', axis=0, tiled=True)  23.6 us
    all_gather x1, blocking collectives, local(): all_weights = lax.all_gather(route_weights, 'ep', axis=0, tiled=True)  23.2 us
    dot_general x1, matrix products, expert_rows(): pre_gate = jnp.dot(picked, gate_proj[0], preferred_element_type=jnp.float32)  13.9 us
    gather x1, local copies, waits for them, and re-layouts, local(): spread_back = jnp.take(results, slot_row, axis=0) * slot_weight[:, None]  12.5 us
    gather x1, local copies, waits for them, and re-layouts, local(): picked = jnp.take(gathered, row_source, axis=0)  11.7 us
    unnamed x1, blocking collectives  7.11 us
  transfers between devices with their start and end apart: 2, of which 1 were waited for; matrix products, arithmetic and copies ran while one was open for 8% of the time, Pallas kernels for 0%

commit v1 on v0

v1 whole, which is shorter than its diff:
```python
import functools
import jax
import jax.numpy as jnp
from jax import lax
from jax.experimental import pallas as pl
from jax.experimental.pallas import tpu as pltpu
from jax.sharding import PartitionSpec as P

SPLIT = 4
TOP = 2
SPAN = 8
MEAN_LIVE = 3

RESIDUAL_SCALE = 8.0**0.25
NORM_EPS = 1e-05
MESH = pl.DeviceIdType.MESH
CHUNKS = 2


def ring_chip(place, chips):
    half = chips // 2
    far = place // half
    return (1 - far) * 2 * place + far * (2 * (chips - 1 - place) + 1)


def ring_place(chip, chips):
    depth, side = chip // 2, chip % 2
    return (1 - side) * depth + side * (chips - 1 - depth)


def neighbourhood(devices):
    chips = devices // 2
    me = lax.axis_index("ep")
    core = me % 2
    place = ring_place(me // 2, chips)
    right = ring_chip((place + 1) % chips, chips) * 2 + core
    left = ring_chip((place + chips - 1) % chips, chips) * 2 + core
    mate = me + 1 - 2 * core
    return chips, me, core, place, (right, left), mate


def greet(others):
    barrier = pltpu.get_barrier_semaphore()
    for other in others:
        pl.semaphore_signal(barrier, inc=1, device_id={"ep": other}, device_id_type=MESH)
    pl.semaphore_wait(barrier, len(others))


def gather_kernel(
    devices, x_ref, m_ref, out_ref, meta_ref,
    send, recv, mate_send, mate_recv, msend, mrecv, mmate_send, mmate_recv, own_sem,
):
    chips, me, core, place, sides, mate = neighbourhood(devices)
    rows = x_ref.shape[0]
    part = rows // 2
    piece = part // CHUNKS
    greet((*sides, mate))

    def remote(src, dst, s_sem, r_sem, device):
        return pltpu.make_async_remote_copy(
            src_ref=src, dst_ref=dst, send_sem=s_sem, recv_sem=r_sem,
            device_id={"ep": device}, device_id_type=MESH,
        )

    def block_at(way, step):
        shift = chips - step if way == 0 else step
        return ring_chip((place + shift) % chips, chips) * 2 + core

    def hop(way, k, step, first=False):
        block = block_at(way, step)
        span = pl.ds(way * part + k * piece, piece)
        src = x_ref.at[span] if first else out_ref.at[block, span]
        return remote(
            src, out_ref.at[block, span], send.at[step, way, k], recv.at[step, way, k], sides[way]
        )

    def share(way, step):
        block = block_at(way, step + 1)
        span = pl.ds(way * part, part)
        view = out_ref.at[block, span]
        return remote(view, view, mate_send.at[step, way], mate_recv.at[step, way], mate)

    def meta_hop(step, first=False):
        block = block_at(0, step)
        src = m_ref if first else meta_ref.at[block]
        return remote(src, meta_ref.at[block], msend.at[step], mrecv.at[step], sides[0])

    def meta_share(step):
        view = meta_ref.at[block_at(0, step + 1)]
        return remote(view, view, mmate_send.at[step], mmate_recv.at[step], mate)

    last = chips - 1
    meta_hop(0, True).start()
    for k in range(CHUNKS):
        for way in range(2):
            hop(way, k, 0, True).start()
    own = pltpu.make_async_copy(x_ref, out_ref.at[me], own_sem.at[0])
    own_meta = pltpu.make_async_copy(m_ref, meta_ref.at[me], own_sem.at[1])
    own.start()
    own_meta.start()
    own_share = remote(
        x_ref, out_ref.at[me], mate_send.at[last, 0], mate_recv.at[last, 0], mate
    )
    own_meta_share = remote(
        m_ref, meta_ref.at[me], mmate_send.at[last], mmate_recv.at[last], mate
    )
    own_share.start()
    own_meta_share.start()

    def advance(step, onward):
        meta_hop(step).wait_recv()
        if onward:
            meta_hop(step + 1).start()
        meta_share(step).start()
        for k in range(CHUNKS):
            for way in range(2):
                hop(way, k, step).wait_recv()
                if onward:
                    hop(way, k, step + 1).start()
        for way in range(2):
            share(way, step).start()

    @pl.loop(0, chips - 2)
    def _(step):
        advance(step, True)

    advance(chips - 2, False)

    @pl.loop(0, chips - 1)
    def _(step):
        meta_hop(step).wait_send()
        meta_share(step).wait()
        for way in range(2):
            for k in range(CHUNKS):
                hop(way, k, step).wait_send()
            share(way, step).wait()

    own.wait()
    own_meta.wait()
    own_share.wait()
    own_meta_share.wait()


def gather_all(tokens, meta, devices):
    rows, width = tokens.shape
    chips = devices // 2
    vmem = pl.BlockSpec(memory_space=pltpu.VMEM)
    dma = pltpu.SemaphoreType.DMA
    return pl.pallas_call(
        functools.partial(gather_kernel, devices),
        out_shape=(
            jax.ShapeDtypeStruct((devices, rows, width), tokens.dtype),
            jax.ShapeDtypeStruct((devices, *meta.shape), meta.dtype),
        ),
        in_specs=[vmem, vmem],
        out_specs=(vmem, vmem),
        scratch_shapes=[
            dma((chips - 1, 2, CHUNKS)), dma((chips - 1, 2, CHUNKS)),
            dma((chips, 2)), dma((chips, 2)),
            dma((chips - 1,)), dma((chips - 1,)),
            dma((chips,)), dma((chips,)),
            dma((2,)),
        ],
        compiler_params=pltpu.CompilerParams(collective_id=0, has_side_effects=True),
        name="ring_gather",
    )(tokens, meta)


def scatter_kernel(
    devices, y_ref, spread_ref, tokens_ref, alive_ref, gain_ref, bias_ref, out_ref,
    mate_sum, high, low, stage, inbox, final, landed,
    swap_send, swap_recv, send, recv, final_send, final_recv,
):
    chips, me, core, place, sides, mate = neighbourhood(devices)
    rows, width = tokens_ref.shape
    half = width // 2
    quarter = half // 2
    greet((*sides, mate))
    here = pl.ds(pl.multiple_of(core * half, half), half)
    there = pl.ds(pl.multiple_of((1 - core) * half, half), half)

    def remote(src, dst, s_sem, r_sem, device):
        return pltpu.make_async_remote_copy(
            src_ref=src, dst_ref=dst, send_sem=s_sem, recv_sem=r_sem,
            device_id={"ep": device}, device_id_type=MESH,
        )

    swap = remote(y_ref.at[:, there], mate_sum, swap_send, swap_recv, mate)
    swap.start()
    swap.wait()
    total = y_ref[:, here] + mate_sum[...]
    top = total.astype(jnp.bfloat16)
    high[...] = top
    low[...] = (total - top.astype(jnp.float32)).astype(jnp.bfloat16)

    def local_part(way, k, step):
        shift = chips - 1 - step if way == 0 else 1 + step
        chip = ring_chip((place + shift) % chips, chips)
        start = pl.multiple_of((chip * 2 + k) * rows, rows)
        picks = spread_ref[pl.ds(start, rows), :]
        columns = pl.ds(way * quarter, quarter)
        return jnp.dot(
            picks, high[:, columns], preferred_element_type=jnp.float32
        ) + jnp.dot(picks, low[:, columns], preferred_element_type=jnp.float32)

    def hop(way, k, step):
        return remote(
            stage.at[step, way, k], inbox.at[step, way, k],
            send.at[step, way, k], recv.at[step, way, k], sides[way],
        )

    for k in range(2):
        for way in range(2):
            stage[0, way, k] = local_part(way, k, 0).astype(jnp.bfloat16)
            hop(way, k, 0).start()

    @pl.loop(1, chips - 1)
    def _(step):
        for k in range(2):
            for way in range(2):
                mine = local_part(way, k, step)
                hop(way, k, step - 1).wait_recv()
                stage[step, way, k] = (
                    mine + inbox[step - 1, way, k].astype(jnp.float32)
                ).astype(jnp.bfloat16)
                hop(way, k, step).start()

    for k in range(2):
        for way in range(2):
            mine = local_part(way, k, chips - 1)
            hop(way, k, chips - 2).wait_recv()
            final[k, :, way * quarter:(way + 1) * quarter] = (
                mine + inbox[chips - 2, way, k].astype(jnp.float32)
            )
    give = remote(final.at[1 - core], landed, final_send, final_recv, mate)
    give.start()

    @pl.loop(0, chips - 1)
    def _(step):
        for k in range(2):
            for way in range(2):
                hop(way, k, step).wait_send()

    give.wait()
    ours = final[core]
    theirs = landed[...]
    first = core == 0
    branch = jnp.concatenate(
        [jnp.where(first, ours, theirs), jnp.where(first, theirs, ours)], axis=1
    )
    values = RESIDUAL_SCALE * tokens_ref[...].astype(jnp.float32) + branch
    center = values - jnp.mean(values, -1, keepdims=True)
    variance = jnp.mean(center * center, -1, keepdims=True)
    normed = center * lax.rsqrt(variance + NORM_EPS) * gain_ref[...] + bias_ref[...]
    out_ref[...] = jnp.where(alive_ref[...] > 0, normed, 0.0).astype(jnp.bfloat16)


def scatter_norm(y, spread, tokens, alive, gain, bias, devices):
    rows, width = tokens.shape
    live = y.shape[0]
    chips = devices // 2
    half, quarter = width // 2, width // 4
    vmem = pl.BlockSpec(memory_space=pltpu.VMEM)
    dma = pltpu.SemaphoreType.DMA
    return pl.pallas_call(
        functools.partial(scatter_kernel, devices),
        out_shape=jax.ShapeDtypeStruct((rows, width), jnp.bfloat16),
        in_specs=[vmem] * 6,
        out_specs=vmem,
        scratch_shapes=[
            pltpu.VMEM((live, half), jnp.float32),
            pltpu.VMEM((live, half), jnp.bfloat16),
            pltpu.VMEM((live, half), jnp.bfloat16),
            pltpu.VMEM((chips - 1, 2, 2, rows, quarter), jnp.bfloat16),
            pltpu.VMEM((chips - 1, 2, 2, rows, quarter), jnp.bfloat16),
            pltpu.VMEM((2, rows, half), jnp.float32),
            pltpu.VMEM((rows, half), jnp.float32),
            dma, dma,
            dma((chips - 1, 2, 2)), dma((chips - 1, 2, 2)),
            dma, dma,
        ],
        compiler_params=pltpu.CompilerParams(
            collective_id=1, has_side_effects=True, vmem_limit_bytes=48 * 1024 * 1024
        ),
        name="ring_scatter_norm",
    )(y, spread, tokens, alive, gain, bias)


def local(
    tokens, lengths, experts, route_weights, gate_proj, up_proj, down_proj, norm_gain, norm_bias
):
    rows, width = tokens.shape
    devices = lax.axis_size("ep")
    expert_count = devices // SPLIT
    seqs = lengths.shape[0]
    live = MEAN_LIVE * seqs * devices
    alive = (jnp.arange(SPAN, dtype=jnp.int32)[None, :] < lengths[:, None]).reshape(rows)
    meta_rows = -(-(expert_count + 1) // 8) * 8
    ids = jnp.arange(meta_rows, dtype=jnp.int32)
    named = experts.T[None, :, :] == ids[:, None, None]
    mixing = jnp.sum(jnp.where(named, route_weights.T[None, :, :], 0.0), axis=1)
    mixing = jnp.where(ids[:, None] == expert_count, 1.0, mixing)
    meta = jnp.where(alive[None, :], mixing, 0.0)
    meta = jnp.pad(meta, ((0, 0), (0, -rows % 128)))
    gathered, metas = gather_all(tokens, meta, devices)
    gathered = gathered.reshape(devices * rows, width)
    own_expert = lax.axis_index("ep") // SPLIT
    weights = lax.dynamic_index_in_dim(metas, own_expert, 1, keepdims=False)[:, :rows]
    living = metas[:, expert_count, :rows]
    upto = jnp.arange(rows)[:, None] <= jnp.arange(rows)[None, :]
    within = jnp.dot(
        living.astype(jnp.bfloat16), upto.astype(jnp.bfloat16),
        preferred_element_type=jnp.float32,
    )
    counts = within[:, -1]
    before = jnp.sum(
        jnp.where(jnp.arange(devices)[:, None] > jnp.arange(devices)[None, :], counts[None, :], 0.0),
        axis=1,
    )
    rank = (within + before[:, None] - 1.0).astype(jnp.int32)
    rank = jnp.where(living > 0, rank, -1).reshape(devices * rows)
    places = jnp.arange(live, dtype=jnp.int32)
    match = rank[None, :] == places[:, None]
    weight = jnp.sum(jnp.where(match, weights.reshape(-1)[None, :], 0.0), axis=1)
    picked = jnp.dot(
        match.astype(jnp.bfloat16), gathered, preferred_element_type=jnp.float32
    ).astype(jnp.bfloat16)
    pre_gate = jnp.dot(picked, gate_proj[0], preferred_element_type=jnp.float32)
    pre_up = jnp.dot(picked, up_proj[0], preferred_element_type=jnp.float32)
    hidden = (jax.nn.silu(pre_gate) * pre_up).astype(jnp.bfloat16)
    y = jnp.dot(hidden, down_proj[0], preferred_element_type=jnp.float32) * weight[:, None]
    spread = (rank[:, None] == places[None, :]).astype(jnp.bfloat16)
    return scatter_norm(
        y, spread, tokens, alive.astype(jnp.float32)[:, None],
        norm_gain[None, :], norm_bias[None, :], devices,
    )


def solution(mesh):
    in_specs = (
        P(("grp", "ep"), None),
        P(("grp", "ep")),
        P(("grp", "ep"), None),
        P(("grp", "ep"), None),
        P("ep", None, None),
        P("ep", None, None),
        P("ep", None, None),
        P(),
        P(),
    )
    out_specs = P(("grp", "ep"), None)
    return jax.shard_map(local, mesh=mesh, in_specs=in_specs, out_specs=out_specs, check_vma=False)
```

time: 261 us -> 103 us (0.39)
  waiting for transfers between devices: 95.3 us -> 0 us
  Pallas kernels: 0 us -> 71.4 us
  blocking collectives: 53.9 us -> 0 us
  local copies, waits for them, and re-layouts: 36.4 us -> 5.77 us
  matrix products: 40.8 us -> 22 us
  other arithmetic: 20 us -> 3.9 us
  between operations: 14.3 us -> 0.08 us
    reduce_scatter x1 -> x0, waiting for transfers between devices: 94.5 us -> none  [local(): lax.psum_scatter(spread_back, 'ep', scatter_dimension=0, tiled=True)]
    pallas_call x0 -> x2, Pallas kernels: none -> 71.4 us  [the longest x1 37.1 us: gather_all(): pl.pallas_call(functools.partial(gather_kernel, devices), out_shape=(jax....]
    all_gather x2 -> x0, blocking collectives: 46.8 us -> none  [the longest x1 23.6 us: local(): lax.all_gather(experts, 'ep', axis=0, tiled=True)]
    gather x4 -> x0, local copies, waits for them, and re-layouts: 31.4 us -> none  [the longest x1 12.5 us: local(): spread_back = jnp.take(results, slot_row, axis=0) * slot_weight[:, None]]
    dot_general x2 -> x4, matrix products: 40.8 us -> 22 us  [the longest x1 13.1 us: local(): jnp.dot(hidden, down_proj[0], preferred_element_type=jnp.float32)]
    unnamed x1 -> x0, blocking collectives: 7.11 us -> none
    mul x1 -> x0, other arithmetic: 5.98 us -> none  [local(): spread_back = jnp.take(results, slot_row, axis=0) * slot_weight[:, None]]
    lt x2 -> x0, other arithmetic: 5.84 us -> none  [the longest x1 5.07 us: local(): position % SPAN < jnp.repeat(lengths, SPAN, total_repeat_length=slot_count)]
  transfers between devices with their start and end apart: 2 -> 0, of which waited for: 1 -> 0; matrix products, arithmetic and copies ran while one was open for 8% -> 0% of each run, Pallas kernels for 0% -> 0%
where the time goes in v1:
time: 103 us
  Pallas kernels  71.4 us (69%)
  matrix products  22 us (21%)
  local copies, waits for them, and re-layouts  5.77 us (6%)
  other arithmetic  3.9 us (4%)
    pallas_call x1, Pallas kernels, gather_all(): pl.pallas_call(functools.partial(gather_kernel, devices), out_shape=(jax....  37.1 us
    pallas_call x1, Pallas kernels, scatter_norm(): pl.pallas_call(functools.partial(scatter_kernel, devices), out_shape=jax....  34.3 us
    dot_general x1, matrix products, local(): jnp.dot(hidden, down_proj[0], preferred_element_type=jnp.float32)  13.1 us
    dot_general x1, matrix products, local(): pre_gate = jnp.dot(picked, gate_proj[0], preferred_element_type=jnp.float32)  4.62 us
    dot_general x1, matrix products, local(): jnp.dot(match.astype(jnp.bfloat16), gathered, preferred_element_type=jnp....  4.14 us
    unnamed x13, local copies, waits for them, and re-layouts  2.98 us

profile of v1, /device:TPU:0, one launch (start us, length us, event | category | flops | bytes accessed | tf_op | source)
XLA Modules:
  0.0 103.1 jit_solution(2883317419362044145)
XLA Ops:
  0.0 0.7 fusion.23
  0.7 0.1 lt.36
  0.8 0.7 select_reduce_fusion.2
  1.5 0.1 select_select_fusion
  1.6 0.6 pad.4.m_ref
  2.2 37.1 %ring_gather.1 = (bf16[16,64,2048]{2,1,0:T(8,128)(2,1)}, f32[16,8,128]{2,1,0:T(8,128)}) custom-call(bf16[64,2048]{1,0:T(8,128)(2,1)} %tokens_ref.1, f32[8,128]{1,0:T(8,128)} %pad.4.m_ref), custom_call_target="tpu_custom_call" | custom-call | tf_op jit(solution)/shard_map/ring_gather/pallas_call | solution.py:149
  39.3 0.9 constant_dynamic-slice_fusion
  40.1 0.1 broadcast_in_dim.99
  40.2 0.8 slice.17
  41.1 0.1 fusion.19
  41.2 0.2 slice_reduce_fusion
  41.4 0.1 select_reduce_fusion.1
  41.5 0.9 slice_compare_fusion
  42.4 0.1 convert_select_fusion
  42.4 0.1 eq.53
  42.5 0.2 select_reduce_fusion
  42.8 0.0 copy-start.4
  42.8 4.1 %convolution_convert_fusion = bf16[384,2048]{1,0:T(8,128)(2,1)S(1)} fusion(bf16[1024,2048]{1,0:T(8,128)(2,1)} %bitcast.37, s32[1024]{0:T(1024)S(1)} %eq.53), kind=kOutput, calls=%fused_computation.8 | convolution fusion | flops 1611792384 | bytes 5771264 | tf_op jit(solution)/shard_map/dot_general | solution.py:325
  46.9 0.0 copy-start.5
  46.9 1.1 %copy-done.5 = bf16[384,2048]{1,0:T(8,128)(2,1)} copy-done((bf16[384,2048]{1,0:T(8,128)(2,1)}, bf16[384,2048]{1,0:T(8,128)(2,1)S(1)}, u32[]{:S(2)}) %copy-start.5) | copy-done | bytes 1572888
  48.1 0.0 copy-done.4
  48.1 4.6 %fusion.4 = f32[384,1792]{1,0:T(8,128)} fusion(bf16[384,2048]{1,0:T(8,128)(2,1)S(1)} %convolution_convert_fusion, bf16[1,2048,1792]{2,1,0:T(8,128)(2,1)S(1)} %copy-done.4), kind=kOutput, calls=%fused_computation.4 | convolution fusion | flops 2818572288 | bytes 11665408 | tf_op jit(solution)/shard_map/dot_general | solution.py:328
  52.7 0.0 copy-start.1
  52.7 0.0 copy-start.2
  52.7 0.0 copy-start.3
  52.7 13.1 %fusion.9.y_ref = f32[384,2048]{1,0:T(8,128)S(1)} fusion(bf16[1,1792,2048]{2,1,0:T(8,128)(2,1)} %param.15, f32[384]{0:T(512)S(1)} %select_reduce_fusion, bf16[384,2048]{1,0:T(8,128)(2,1)} %copy-done.5, bf16[1,2048,1792]{2,1,0:T(8,128)(2,1)} %param.14, f32[384,1792]{1,0:T(8,128)} %fusion.4), kind=kOutput, calls=%fused_computation.7 | convolution fusion | flops 5642059776 | bytes 22152704 | tf_op jit(solution)/shard_map/dot_general | solution.py:331
  65.8 1.1 %fusion.15.spread_ref = bf16[1024,384]{1,0:T(8,128)(2,1)} fusion(s32[1024]{0:T(1024)S(1)} %eq.53), kind=kLoop, calls=%fused_computation.13 | loop fusion | flops 786432 | bytes 790528 | tf_op jit(solution)/shard_map/convert_element_type | solution.py:332
  66.9 0.1 reshape.62.alive_ref
  67.0 0.0 copy-done.1
  67.0 0.0 copy-done.2
  67.0 0.0 copy-done.3
  67.0 0.0 copy-start
  67.0 1.1 %copy-done = bf16[1024,384]{1,0:T(8,128)(2,1)S(1)} copy-done((bf16[1024,384]{1,0:T(8,128)(2,1)S(1)}, bf16[1024,384]{1,0:T(8,128)(2,1)}, u32[]{:S(2)}) %copy-start) | copy-done | bytes 786456
  68.1 34.3 %ring_scatter_norm.1 = bf16[64,2048]{1,0:T(8,128)(2,1)S(1)} custom-call(f32[384,2048]{1,0:T(8,128)S(1)} %fusion.9.y_ref, bf16[1024,384]{1,0:T(8,128)(2,1)S(1)} %copy-done, bf16[64,2048]{1,0:T(8,128)(2,1)S(1)} %copy-done.1, f32[64,1]{1,0:T(8,128)S(1)} %reshape.62.alive_ref, f32[1,2048]{1,0:T(1,128)S(1)} %bitcast.32, f32[1,2048]{1,0:T(1,128)S(1)} %bitcast.33), custom_call_target="tpu_custom_call" | custom-call | tf_op jit(solution)/shard_map/ring_scatter_norm/pallas_call | solution.py:265
  102.4 0.7 copy.21
  (1 shorter events, 0.0 us)
Async XLA Ops:
  42.8 5.3 %copy-start.4 = (bf16[1,2048,1792]{2,1,0:T(8,128)(2,1)S(1)}, bf16[1,2048,1792]{2,1,0:T(8,128)(2,1)}, u32[]{:S(2)}) copy-start(bf16[1,2048,1792]{2,1,0:T(8,128)(2,1)} %param.13) | copy-start | bytes 22020100
  46.9 1.1 %copy-start.5 = (bf16[384,2048]{1,0:T(8,128)(2,1)}, bf16[384,2048]{1,0:T(8,128)(2,1)S(1)}, u32[]{:S(2)}) copy-start(bf16[384,2048]{1,0:T(8,128)(2,1)S(1)} %convolution_convert_fusion) | copy-start | bytes 4718596
  52.7 14.3 %copy-start.1 = (bf16[64,2048]{1,0:T(8,128)(2,1)S(1)}, bf16[64,2048]{1,0:T(8,128)(2,1)}, u32[]{:S(2)}) copy-start(bf16[64,2048]{1,0:T(8,128)(2,1)} %tokens_ref.1) | copy-start | bytes 786436
  52.7 14.3 %copy-start.2 = (f32[2048]{0:T(1024)S(1)}, f32[2048]{0:T(1024)}, u32[]{:S(2)}) copy-start(f32[2048]{0:T(1024)} %param.16) | copy-start | bytes 24580
  52.7 14.3 %copy-start.3 = (f32[2048]{0:T(1024)S(1)}, f32[2048]{0:T(1024)}, u32[]{:S(2)}) copy-start(f32[2048]{0:T(1024)} %param.17) | copy-start | bytes 24580
  67.0 1.1 %copy-start = (bf16[1024,384]{1,0:T(8,128)(2,1)S(1)}, bf16[1024,384]{1,0:T(8,128)(2,1)}, u32[]{:S(2)}) copy-start(bf16[1024,384]{1,0:T(8,128)(2,1)} %fusion.15.spread_ref) | copy-start | bytes 2359300

commit v2 on v1

v2 whole, which is shorter than its diff:
```python
import functools
import jax
import jax.numpy as jnp
from jax import lax
from jax.experimental import pallas as pl
from jax.experimental.pallas import tpu as pltpu
from jax.sharding import PartitionSpec as P

SPLIT = 4
TOP = 2
SPAN = 8
MEAN_LIVE = 3

RESIDUAL_SCALE = 8.0**0.25
NORM_EPS = 1e-05
MESH = pl.DeviceIdType.MESH
CHUNKS = 4


def ring_chip(place, chips):
    half = chips // 2
    far = place // half
    return (1 - far) * 2 * place + far * (2 * (chips - 1 - place) + 1)


def ring_place(chip, chips):
    depth, side = chip // 2, chip % 2
    return (1 - side) * depth + side * (chips - 1 - depth)


def neighbourhood(devices):
    chips = devices // 2
    me = lax.axis_index("ep")
    core = me % 2
    place = ring_place(me // 2, chips)
    right = ring_chip((place + 1) % chips, chips) * 2 + core
    left = ring_chip((place + chips - 1) % chips, chips) * 2 + core
    mate = me + 1 - 2 * core
    return chips, me, core, place, (right, left), mate


def greet(others):
    barrier = pltpu.get_barrier_semaphore()
    for other in others:
        pl.semaphore_signal(barrier, inc=1, device_id={"ep": other}, device_id_type=MESH)
    pl.semaphore_wait(barrier, len(others))


def remote(src, dst, s_sem, r_sem, device):
    return pltpu.make_async_remote_copy(
        src_ref=src, dst_ref=dst, send_sem=s_sem, recv_sem=r_sem,
        device_id={"ep": device}, device_id_type=MESH,
    )


def layer_kernel(
    devices, expert_count,
    x_ref, m_ref, gate_hbm, up_hbm, down_hbm, alive_ref, gain_ref, bias_ref, out_ref,
    all_x, all_meta, gate_ref, up_ref, down_ref,
    chip_meta, living, match_ref, spread_ref, picked, hidden, mate_give, mate_sum, mine_y,
    stage, inbox, final, landed,
    weight_sem, send, recv, mate_send, mate_recv, msend, mrecv, mmate_send, mmate_recv, own_sem,
    swap_send, swap_recv, rsend, rrecv, final_send, final_recv,
):
    chips, me, core, place, sides, mate = neighbourhood(devices)
    rows, width = x_ref.shape
    live = picked.shape[0]
    hidden_units = hidden.shape[1]
    part = rows // 2
    piece = width // CHUNKS
    half = width // 2
    quarter = half // 2
    loads = [
        pltpu.make_async_copy(gate_hbm.at[0], gate_ref, weight_sem.at[0]),
        pltpu.make_async_copy(up_hbm.at[0], up_ref, weight_sem.at[1]),
        pltpu.make_async_copy(down_hbm.at[0], down_ref, weight_sem.at[2]),
    ]
    greet((*sides, mate))

    def block_at(way, step):
        shift = chips - step if way == 0 else step
        return ring_chip((place + shift) % chips, chips) * 2 + core

    def hop(way, k, step, first=False):
        block = block_at(way, step)
        span, columns = pl.ds(way * part, part), pl.ds(k * piece, piece)
        src = x_ref.at[span, columns] if first else all_x.at[block, span, columns]
        return remote(
            src, all_x.at[block, span, columns],
            send.at[step, way, k], recv.at[step, way, k], sides[way],
        )

    def share(way, step):
        view = all_x.at[block_at(way, step + 1), pl.ds(way * part, part)]
        return remote(view, view, mate_send.at[step, way], mate_recv.at[step, way], mate)

    def meta_hop(step, first=False):
        block = block_at(0, step)
        src = m_ref if first else all_meta.at[block]
        return remote(src, all_meta.at[block], msend.at[step], mrecv.at[step], sides[0])

    def meta_share(step):
        view = all_meta.at[block_at(0, step + 1)]
        return remote(view, view, mmate_send.at[step], mmate_recv.at[step], mate)

    last = chips - 1
    meta_hop(0, True).start()
    for k in range(CHUNKS):
        for way in range(2):
            hop(way, k, 0, True).start()
    own = pltpu.make_async_copy(x_ref, all_x.at[me], own_sem.at[0])
    own_meta = pltpu.make_async_copy(m_ref, all_meta.at[me], own_sem.at[1])
    own.start()
    own_meta.start()
    own_share = remote(x_ref, all_x.at[me], mate_send.at[last, 0], mate_recv.at[last, 0], mate)
    own_meta_share = remote(
        m_ref, all_meta.at[me], mmate_send.at[last], mmate_recv.at[last], mate
    )
    own_share.start()
    own_meta_share.start()
    for load in loads:
        load.start()

    def advance(step, onward):
        meta_hop(step).wait_recv()
        if onward:
            meta_hop(step + 1).start()
        meta_share(step).start()
        for k in range(CHUNKS):
            for way in range(2):
                hop(way, k, step).wait_recv()
                if onward:
                    hop(way, k, step + 1).start()
        for way in range(2):
            share(way, step).start()

    @pl.loop(0, chips - 2)
    def _(step):
        advance(step, True)

    advance(chips - 2, False)

    @pl.loop(0, chips - 1)
    def _(step):
        meta_hop(step).wait_send()
        meta_share(step).wait()
        for way in range(2):
            for k in range(CHUNKS):
                hop(way, k, step).wait_send()
            share(way, step).wait()

    own.wait()
    own_meta.wait()
    own_share.wait()
    own_meta_share.wait()

    lanes = 2 * rows
    for q in range(chips):
        pair = all_meta[2 * q] + all_meta[2 * q + 1]
        chip_meta[q] = pair
        living[q:q + 1, :] = pair[expert_count:expert_count + 1, :]
    lives = living[...]
    upto = (
        lax.broadcasted_iota(jnp.int32, (lanes, lanes), 0)
        <= lax.broadcasted_iota(jnp.int32, (lanes, lanes), 1)
    )
    within = jnp.dot(lives, upto.astype(jnp.float32), preferred_element_type=jnp.float32)
    own_expert = me // SPLIT
    line = lax.broadcasted_iota(jnp.int32, (live, lanes), 0).astype(jnp.float32)
    weight_sum = jnp.zeros((live, lanes), jnp.float32)
    before = jnp.full((1, 1), -1.0, jnp.float32)
    for q in range(chips):
        lived = lives[q:q + 1, :]
        rank = jnp.where(lived > 0, within[q:q + 1, :] + before, -1.0)
        before = before + jnp.sum(lived, 1, keepdims=True)
        same = line == rank
        weight_sum += jnp.where(same, chip_meta[q, pl.ds(own_expert, 1), :], 0.0)
        ones = same.astype(jnp.float32)
        match_ref[:, q * lanes:(q + 1) * lanes] = ones.astype(jnp.bfloat16)
        spread_ref[q * lanes:(q + 1) * lanes, :] = jnp.transpose(ones).astype(jnp.bfloat16)
    weight = jnp.sum(weight_sum, 1, keepdims=True)

    tile = 256

    @pl.loop(0, width // tile)
    def _(t):
        columns = pl.ds(pl.multiple_of(t * tile, tile), tile)
        rows_all = all_x[:, :, columns].reshape(devices * rows, tile)
        picked[:, columns] = jnp.dot(
            match_ref[...], rows_all, preferred_element_type=jnp.float32
        ).astype(jnp.bfloat16)

    for load in loads[:2]:
        load.wait()

    @pl.loop(0, hidden_units // tile)
    def _(t):
        columns = pl.ds(pl.multiple_of(t * tile, tile), tile)
        g = jnp.dot(picked[...], gate_ref[:, columns], preferred_element_type=jnp.float32)
        u = jnp.dot(picked[...], up_ref[:, columns], preferred_element_type=jnp.float32)
        hidden[:, columns] = (jax.nn.silu(g) * u).astype(jnp.bfloat16)

    loads[2].wait()

    def down_into(base, dst):
        @pl.loop(0, half // tile)
        def _(t):
            columns = pl.ds(pl.multiple_of(t * tile, tile), tile)
            source = pl.ds(pl.multiple_of(base + t * tile, tile), tile)
            dst[:, columns] = weight * jnp.dot(
                hidden[...], down_ref[:, source], preferred_element_type=jnp.float32
            )

    down_into((1 - core) * half, mate_give)
    swap = remote(mate_give, mate_sum, swap_send, swap_recv, mate)
    swap.start()
    down_into(core * half, mine_y)
    swap.wait()
    total = mine_y[...] + mate_sum[...]
    top = total.astype(jnp.bfloat16)
    high, low = picked.at[:, pl.ds(0, half)], picked.at[:, pl.ds(half, half)]
    high[...] = top
    low[...] = (total - top.astype(jnp.float32)).astype(jnp.bfloat16)

    cut = lanes // CHUNKS

    def local_part(way, step):
        shift = chips - 1 - step if way == 0 else 1 + step
        chip = ring_chip((place + shift) % chips, chips)
        picks = spread_ref[pl.ds(pl.multiple_of(chip * lanes, lanes), lanes), :]
        columns = pl.ds(way * quarter, quarter)
        return jnp.dot(
            picks, high[:, columns], preferred_element_type=jnp.float32
        ) + jnp.dot(picks, low[:, columns], preferred_element_type=jnp.float32)

    def pass_on(way, k, step):
        return remote(
            stage.at[step, way, k], inbox.at[step, way, k],
            rsend.at[step, way, k], rrecv.at[step, way, k], sides[way],
        )

    for way in range(2):
        part_sum = local_part(way, 0)
        for k in range(CHUNKS):
            stage[0, way, k] = part_sum[k * cut:(k + 1) * cut].astype(jnp.bfloat16)
            pass_on(way, k, 0).start()

    @pl.loop(1, chips - 1)
    def _(step):
        sums = [local_part(way, step) for way in range(2)]
        for k in range(CHUNKS):
            for way in range(2):
                pass_on(way, k, step - 1).wait_recv()
                stage[step, way, k] = (
                    sums[way][k * cut:(k + 1) * cut]
                    + inbox[step - 1, way, k].astype(jnp.float32)
                ).astype(jnp.bfloat16)
                pass_on(way, k, step).start()

    sums = [local_part(way, chips - 1) for way in range(2)]
    for k in range(CHUNKS):
        for way in range(2):
            pass_on(way, k, chips - 2).wait_recv()
            final[k * cut:(k + 1) * cut, way * quarter:(way + 1) * quarter] = (
                sums[way][k * cut:(k + 1) * cut]
                + inbox[chips - 2, way, k].astype(jnp.float32)
            )
    theirs_at = pl.ds(pl.multiple_of((1 - core) * rows, rows), rows)
    ours_at = pl.ds(pl.multiple_of(core * rows, rows), rows)
    give = remote(final.at[theirs_at], landed, final_send, final_recv, mate)
    give.start()

    @pl.loop(0, chips - 1)
    def _(step):
        for k in range(CHUNKS):
            for way in range(2):
                pass_on(way, k, step).wait_send()

    give.wait()
    ours = final[ours_at, :]
    theirs = landed[...]
    first = core == 0
    branch = jnp.concatenate(
        [jnp.where(first, ours, theirs), jnp.where(first, theirs, ours)], axis=1
    )
    values = RESIDUAL_SCALE * x_ref[...].astype(jnp.float32) + branch
    center = values - jnp.mean(values, -1, keepdims=True)
    variance = jnp.mean(center * center, -1, keepdims=True)
    normed = center * lax.rsqrt(variance + NORM_EPS) * gain_ref[...] + bias_ref[...]
    out_ref[...] = jnp.where(alive_ref[...] > 0, normed, 0.0).astype(jnp.bfloat16)


def whole_layer(tokens, meta, gate, up, down, alive, gain, bias, devices, expert_count, live):
    rows, width = tokens.shape
    chips = devices // 2
    units = gate.shape[2]
    half, quarter = width // 2, width // 4
    vmem = pl.BlockSpec(memory_space=pltpu.VMEM)
    anywhere = pl.BlockSpec(memory_space=pl.ANY)
    dma = pltpu.SemaphoreType.DMA
    bf16, f32 = jnp.bfloat16, jnp.float32
    ring = (chips - 1, 2, CHUNKS)
    return pl.pallas_call(
        functools.partial(layer_kernel, devices, expert_count),
        out_shape=jax.ShapeDtypeStruct((rows, width), bf16),
        in_specs=[vmem, vmem, anywhere, anywhere, anywhere, vmem, vmem, vmem],
        out_specs=vmem,
        scratch_shapes=[
            pltpu.VMEM((devices, rows, width), bf16),
            pltpu.VMEM((devices, *meta.shape), f32),
            pltpu.VMEM(gate.shape[1:], bf16),
            pltpu.VMEM(up.shape[1:], bf16),
            pltpu.VMEM(down.shape[1:], bf16),
            pltpu.VMEM((chips, *meta.shape), f32),
            pltpu.VMEM((chips, 2 * rows), f32),
            pltpu.VMEM((live, devices * rows), bf16),
            pltpu.VMEM((devices * rows, live), bf16),
            pltpu.VMEM((live, width), bf16),
            pltpu.VMEM((live, units), bf16),
            pltpu.VMEM((live, half), f32),
            pltpu.VMEM((live, half), f32),
            pltpu.VMEM((live, half), f32),
            pltpu.VMEM((*ring, 2 * rows // CHUNKS, quarter), bf16),
            pltpu.VMEM((*ring, 2 * rows // CHUNKS, quarter), bf16),
            pltpu.VMEM((2 * rows, half), f32),
            pltpu.VMEM((rows, half), f32),
            dma((3,)),
            dma(ring), dma(ring),
            dma((chips, 2)), dma((chips, 2)),
            dma((chips - 1,)), dma((chips - 1,)),
            dma((chips,)), dma((chips,)),
            dma((2,)),
            dma, dma,
            dma(ring), dma(ring),
            dma, dma,
        ],
        compiler_params=pltpu.CompilerParams(
            collective_id=0, has_side_effects=True, vmem_limit_bytes=67043328
        ),
        name="layer",
    )(tokens, meta, gate, up, down, alive, gain, bias)


def local(
    tokens, lengths, experts, route_weights, gate_proj, up_proj, down_proj, norm_gain, norm_bias
):
    rows, width = tokens.shape
    devices = lax.axis_size("ep")
    expert_count = devices // SPLIT
    seqs = lengths.shape[0]
    live = MEAN_LIVE * seqs * devices
    alive = (jnp.arange(SPAN, dtype=jnp.int32)[None, :] < lengths[:, None]).reshape(rows)
    meta_rows = -(-(expert_count + 1) // 8) * 8
    ids = jnp.arange(meta_rows, dtype=jnp.int32)
    named = experts.T[None, :, :] == ids[:, None, None]
    mixing = jnp.sum(jnp.where(named, route_weights.T[None, :, :], 0.0), axis=1)
    mixing = jnp.where(ids[:, None] == expert_count, 1.0, mixing)
    meta = jnp.where(alive[None, :], mixing, 0.0)
    core = lax.axis_index("ep") % 2
    blank = jnp.zeros_like(meta)
    meta = jnp.where(
        core == 0,
        jnp.concatenate([meta, blank], axis=1),
        jnp.concatenate([blank, meta], axis=1),
    )
    return whole_layer(
        tokens, meta, gate_proj, up_proj, down_proj, alive.astype(jnp.float32)[:, None],
        norm_gain[None, :], norm_bias[None, :], devices, expert_count, live,
    )


def solution(mesh):
    in_specs = (
        P(("grp", "ep"), None),
        P(("grp", "ep")),
        P(("grp", "ep"), None),
        P(("grp", "ep"), None),
        P("ep", None, None),
        P("ep", None, None),
        P("ep", None, None),
        P(),
        P(),
    )
    out_specs = P(("grp", "ep"), None)
    return jax.shard_map(local, mesh=mesh, in_specs=in_specs, out_specs=out_specs, check_vma=False)
```

time: 103 us -> 81.3 us (0.79)
  matrix products: 22 us -> 0 us
  Pallas kernels: 71.4 us -> 76.5 us
  local copies, waits for them, and re-layouts: 5.77 us -> 2.45 us
  other arithmetic: 3.9 us -> 2.18 us
    dot_general x4 -> x0, matrix products: 22 us -> none  [the longest x1 13.1 us: local(): jnp.dot(hidden, down_proj[0], preferred_element_type=jnp.float32)]
    pallas_call x2 -> x1, Pallas kernels: 71.4 us -> 76.5 us  [whole_layer(): pl.pallas_call(functools.partial(layer_kernel, devices, expert_count), ou...]
    unnamed x13 -> x1, local copies, waits for them, and re-layouts: 2.98 us -> 1.67 us
    convert_element_type x1 -> x0, other arithmetic: 1.08 us -> none  [local(): spread = (rank[:, None] == places[None, :]).astype(jnp.bfloat16)]
    slice x2 -> x0, local copies, waits for them, and re-layouts: 1.03 us -> none  [the longest x1 0.85 us: local(): living = metas[:, expert_count, :rows]]
where the time goes in v2:
time: 81.3 us; the launch traced here: 81.1 us
  Pallas kernels  76.5 us (94%)
  local copies, waits for them, and re-layouts  2.45 us (3%)
  other arithmetic  2.18 us (3%)
    pallas_call x1, Pallas kernels, whole_layer(): pl.pallas_call(functools.partial(layer_kernel, devices, expert_count), ou...  76.5 us
    unnamed x1, local copies, waits for them, and re-layouts  1.67 us

profile of v2, /device:TPU:0, one launch (start us, length us, event | category | flops | bytes accessed | tf_op | source)
XLA Modules:
  0.0 81.1 jit_solution(16430606585092464345)
XLA Ops:
  0.0 0.7 select_reduce_fusion
  0.7 0.7 fusion
  1.4 0.1 lt.39
  1.5 0.1 select_select_fusion
  1.6 0.7 pad_select_fusion.m_ref
  2.3 0.7 reshape.49.alive_ref
  3.0 76.5 %layer.1 = bf16[64,2048]{1,0:T(8,128)(2,1)} custom-call(bf16[64,2048]{1,0:T(8,128)(2,1)} %x_ref.1, f32[8,128]{1,0:T(8,128)} %pad_select_fusion.m_ref, bf16[1,2048,1792]{2,1,0:T(8,128)(2,1)} %gate_hbm.1, bf16[1,2048,1792]{2,1,0:T(8,128)(2,1)} %up_hbm.1, bf16[1,1792,2048]{2,1,0:T(8,128)(2,1)} %down_hbm.1, f32[64,1]{1,0:T(8,128)} %reshape.49.alive_ref, ...), custom_call_target="tpu_custom_call" | custom-call | tf_op jit(solution)/shard_map/layer/pallas_call | solution.py:303
  79.4 1.7 %copy.13 = bf16[64,2048]{1,0:T(8,128)(2,1)} copy(bf16[64,2048]{1,0:T(8,128)(2,1)} %layer.1) | data formatting | bytes 524288
  (1 shorter events, 0.0 us)

commit v3 on v2

--- a/solution.py
+++ b/solution.py
@@ -55,7 +55,7 @@
 
 def layer_kernel(
     devices, expert_count,
-    x_ref, m_ref, gate_hbm, up_hbm, down_hbm, alive_ref, gain_ref, bias_ref, out_ref,
+    x_ref, m_ref, gate_hbm, up_hbm, down_hbm, lengths_ref, gain_ref, bias_ref, out_ref,
     all_x, all_meta, gate_ref, up_ref, down_ref,
     chip_meta, living, match_ref, spread_ref, picked, hidden, mate_give, mate_sum, mine_y,
     stage, inbox, final, landed,
@@ -180,7 +180,9 @@
         spread_ref[q * lanes:(q + 1) * lanes, :] = jnp.transpose(ones).astype(jnp.bfloat16)
     weight = jnp.sum(weight_sum, 1, keepdims=True)
 
-    tile = 256
+    tile = 2 * 256
+    slab = hidden_units // 2 if hidden_units % 256 == 0 and devices <= 4 * SPLIT else 256
+    slabs = hidden_units // slab
 
     @pl.loop(0, width // tile)
     def _(t):
@@ -193,9 +195,9 @@
     for load in loads[:2]:
         load.wait()
 
-    @pl.loop(0, hidden_units // tile)
+    @pl.loop(0, slabs)
     def _(t):
-        columns = pl.ds(pl.multiple_of(t * tile, tile), tile)
+        columns = pl.ds(pl.multiple_of(t * slab, slab), slab)
         g = jnp.dot(picked[...], gate_ref[:, columns], preferred_element_type=jnp.float32)
         u = jnp.dot(picked[...], up_ref[:, columns], preferred_element_type=jnp.float32)
         hidden[:, columns] = (jax.nn.silu(g) * u).astype(jnp.bfloat16)
@@ -287,10 +289,16 @@
     center = values - jnp.mean(values, -1, keepdims=True)
     variance = jnp.mean(center * center, -1, keepdims=True)
     normed = center * lax.rsqrt(variance + NORM_EPS) * gain_ref[...] + bias_ref[...]
-    out_ref[...] = jnp.where(alive_ref[...] > 0, normed, 0.0).astype(jnp.bfloat16)
-
-
-def whole_layer(tokens, meta, gate, up, down, alive, gain, bias, devices, expert_count, live):
+    seqs = rows // SPAN
+    offset = lax.broadcasted_iota(jnp.int32, (rows, seqs), 0) - SPAN * lax.broadcasted_iota(
+        jnp.int32, (rows, seqs), 1
+    )
+    lit = jnp.where((offset >= 0) & (offset < lengths_ref[...]), 1.0, 0.0)
+    alive = jnp.sum(lit, axis=1, keepdims=True)
+    out_ref[...] = jnp.where(alive > 0, normed, 0.0).astype(jnp.bfloat16)
+
+
+def whole_layer(tokens, meta, gate, up, down, lengths, gain, bias, devices, expert_count, live):
     rows, width = tokens.shape
     chips = devices // 2
     units = gate.shape[2]
@@ -338,7 +346,7 @@
             collective_id=0, has_side_effects=True, vmem_limit_bytes=67043328
         ),
         name="layer",
-    )(tokens, meta, gate, up, down, alive, gain, bias)
+    )(tokens, meta, gate, up, down, lengths, gain, bias)
 
 
 def local(
@@ -364,7 +372,7 @@
         jnp.concatenate([blank, meta], axis=1),
     )
     return whole_layer(
-        tokens, meta, gate_proj, up_proj, down_proj, alive.astype(jnp.float32)[:, None],
+        tokens, meta, gate_proj, up_proj, down_proj, lengths[None, :],
         norm_gain[None, :], norm_bias[None, :], devices, expert_count, live,
     )
 

time: 81.3 us -> 79.2 us (0.974)
  Pallas kernels: 76.5 us -> 75.1 us
    pallas_call x1, Pallas kernels: 76.5 us -> 75.1 us  [whole_layer(): pl.pallas_call(functools.partial(layer_kernel, devices, expert_count), ou...]
where the time goes in v3:
time: 79.2 us; the launch traced here: 79.1 us
  Pallas kernels  75.1 us (95%)
  other arithmetic  2.18 us (3%)
  local copies, waits for them, and re-layouts  1.76 us (2%)
    pallas_call x1, Pallas kernels, whole_layer(): pl.pallas_call(functools.partial(layer_kernel, devices, expert_count), ou...  75.1 us
    unnamed x1, local copies, waits for them, and re-layouts  1.67 us

profile of v3, /device:TPU:0, one launch (start us, length us, event | category | flops | bytes accessed | tf_op | source)
XLA Modules:
  0.0 79.1 jit_solution(10834401190815460224)
XLA Ops:
  0.0 0.7 iota_compare_fusion.1
  0.7 0.1 lt.30
  0.8 0.7 select_reduce_fusion
  1.5 0.1 select_select_fusion
  1.6 0.7 pad_select_fusion.m_ref
  2.3 75.1 %layer.1 = bf16[64,2048]{1,0:T(8,128)(2,1)} custom-call(bf16[64,2048]{1,0:T(8,128)(2,1)} %x_ref.1, f32[8,128]{1,0:T(8,128)} %pad_select_fusion.m_ref, bf16[1,2048,1792]{2,1,0:T(8,128)(2,1)} %gate_hbm.1, bf16[1,2048,1792]{2,1,0:T(8,128)(2,1)} %up_hbm.1, bf16[1,1792,2048]{2,1,0:T(8,128)(2,1)} %down_hbm.1, s32[1,8]{1,0:T(1,128)} %bitcast.9, f32[1,2048]{1,0:T(1,128)} %bitcast.5, ...), custom_call_target="tpu_custom_call" | custom-call | tf_op jit(solution)/shard_map/layer/pallas_call | solution.py:311
  77.4 1.7 %copy.11 = bf16[64,2048]{1,0:T(8,128)(2,1)} copy(bf16[64,2048]{1,0:T(8,128)(2,1)} %layer.1) | data formatting | bytes 524288
  (1 shorter events, 0.0 us)
